TPU v7x, 256 devices: a whole 4x4x8 slice. The times are simulated.
256 devices in a mesh: gr: 2 (over z_hi), sp: 16 (over z_lo, y), tp: 8 (over x, core).
Axes of the slice: x: 4, y: 4, z: 8 (z_hi: 2, z_lo: 4; z = z_hi * 4 + z_lo), core: 2. Of those that a mesh axis runs over, the one named last changes fastest.
Arguments:
- tokens: bfloat16 [8, 3072, 4096], P('gr', 'sp', 'tp'), may hold values from -6.5 to 6.5
- first_token_input: bfloat16 [8, 4096], P('gr', 'sp'), may hold values from -6 to 6
- forget_weight: bfloat16 [4096, 4096], P(None, 'tp'), may hold values from -0.1171875 to 0.1171875
- value_weight: bfloat16 [4096, 4096], P(None, 'tp'), may hold values from -0.375 to 0.375
- query_weight: bfloat16 [4096, 4096], P('sp', 'tp'), may hold values from -0.09375 to 0.09375
- output_gate_weight: bfloat16 [4096, 4096], P('sp', 'tp'), may hold values from -0.09375 to 0.09375
- forget_bound_slack: float32 [4096], P('tp'), may hold values from 0.00016276042 to 0.8, as said below
- additional_damping_exponent: float32 [8, 3072, 32], P('gr', 'sp', 'tp'), may hold values from -2.2 to 0, as said below
- read_norm_scale: float32 [128], replicated, may hold values from 0.1 to 1.9
Outputs:
- cache: bfloat16 [8, 32, 128, 128], P('gr', 'tp', 'sp')
- first_read: bfloat16 [8, 4096], P('gr', 'tp')
Inputs may be any that keep to these rules, and one draw needn't show every extreme that they name: `forget_bound_slack`: positive gaps, one per channel. `additional_damping_exponent`: non-positive log-decays.
All inputs are finite; a program needn't handle non-finite values.
Results may differ from a plain program's by a relative error of at most 0.018.
Values may be sent and summed in bfloat16 or wider, within the bound.
No kernel may reach another device: no remote copies, remote signals or barrier semaphores. Data moves between devices by JAX's collectives and lax.ppermute only.
A program may use at most 64 MiB of HBM per device.

v0:
```python
import jax
import jax.numpy as jnp
from jax import lax
from jax.sharding import PartitionSpec as P


def from_everyone(shard, axis):
    count = lax.axis_size(axis)
    return lax.all_to_all(
        jnp.broadcast_to(shard[None], (count, *shard.shape)), axis, 0, 0, tiled=True
    )


def folded_in_pairs(pieces, combine):
    while len(jax.tree.leaves(pieces)[0]) > 1:
        pieces = jax.vmap(combine)(*(pieces[side::2] for side in (0, 1)))
    return pieces[0]


def prefix(shard, axis, combine, identity):
    count, position = (lax.axis_size(axis), lax.axis_index(axis))
    passed = jnp.arange(count) > position

    def kept(part, zero, own):
        part = jnp.where(
            passed.reshape(-1, *(1 for _ in own.shape)), part, jnp.asarray(zero, own.dtype)
        )
        return part[::-1]

    pieces = from_everyone(shard, axis)
    return folded_in_pairs(kept(pieces, identity, shard), combine)


def cut_along(shard, dim, count):
    shape = shard.shape
    blocks = shard.reshape(*shape[:dim], count, shape[dim] // count, *shape[dim + 1 :])
    return jnp.moveaxis(blocks, dim, 0)


def sent_and_summed(shard, axis, dim):
    count = lax.axis_size(axis)
    blocks = lax.all_to_all(cut_along(shard, dim, count), axis, 0, 0, tiled=True)
    return jnp.sum(blocks.astype(jnp.float32), axis=0)


def of_everyone(shard, axis):
    everything = from_everyone(shard, axis)
    return jnp.sum(everything, axis=0)


def packed_total(arrays, axis):
    ends = [0]
    for a in arrays:
        ends.append(ends[-1] + a.size)
    total = of_everyone(jnp.concatenate([a.ravel() for a in arrays]), axis)
    return tuple((total[b:e].reshape(a.shape) for a, b, e in zip(arrays, ends, ends[1:])))


def add_sums(earlier, later_part):
    return earlier + later_part


def per_device(
    tokens,
    first_token_input,
    forget_weight,
    value_weight,
    query_weight,
    output_gate_weight,
    forget_bound_slack,
    additional_damping_exponent,
    read_norm_scale,
):
    seq_count, block_len, width_part = tokens.shape
    head_dim = read_norm_scale.shape[0]
    local_heads = additional_damping_exponent.shape[2]
    channels = local_heads * head_dim
    flat_rows = tokens.reshape(seq_count * block_len, width_part)
    segment = lax.all_gather(flat_rows, "tp", axis=1, tiled=True)
    forget_acc = jnp.dot(segment, forget_weight, preferred_element_type=jnp.float32)
    value_acc = jnp.dot(segment, value_weight, preferred_element_type=jnp.float32)
    forget = forget_acc.astype(jnp.bfloat16).reshape(seq_count, block_len, channels)
    values = value_acc.astype(jnp.bfloat16).reshape(seq_count, block_len, local_heads, head_dim)
    sp_count = lax.axis_size("sp")
    rows_here = head_dim // sp_count
    row_start = lax.axis_index("sp") * rows_here
    valve_sampler_seeds = forget_bound_slack * jax.nn.sigmoid(-forget.astype(jnp.float32))
    damping_exponent = jnp.log1p(-valve_sampler_seeds) + jnp.repeat(
        additional_damping_exponent, head_dim, axis=2
    )
    totals = jnp.sum(damping_exponent, axis=1)
    later_sum = prefix(totals, "sp", add_sums, jnp.zeros_like(totals))
    within = totals[:, None, :] - jnp.cumsum(damping_exponent, axis=1)
    weighted = (valve_sampler_seeds * jnp.exp(within + later_sum[:, None, :])).astype(jnp.bfloat16)
    weighted = weighted.reshape(seq_count, block_len, local_heads, head_dim)
    state_terms = jnp.einsum(
        "slha,slhb->shab", weighted, values, preferred_element_type=jnp.float32
    )
    state_sum = sent_and_summed(state_terms.astype(jnp.bfloat16), "sp", 2)
    cache_rows = state_sum.astype(jnp.bfloat16)
    slab_rows = first_token_input.shape[1]
    row_first = lax.axis_index("sp") * slab_rows
    forget_rows = lax.dynamic_slice_in_dim(forget_weight, row_first, slab_rows, 0)
    value_rows = lax.dynamic_slice_in_dim(value_weight, row_first, slab_rows, 0)
    new_sums = packed_total(
        (
            jnp.dot(first_token_input, query_weight, preferred_element_type=jnp.float32),
            jnp.dot(first_token_input, output_gate_weight, preferred_element_type=jnp.float32),
            jnp.dot(first_token_input, forget_rows, preferred_element_type=jnp.float32),
            jnp.dot(first_token_input, value_rows, preferred_element_type=jnp.float32),
        ),
        "sp",
    )
    new_query, new_gate, new_forget, new_value = [
        summed.astype(jnp.bfloat16) for summed in new_sums
    ]
    new_keys = (forget_bound_slack * jax.nn.sigmoid(-new_forget.astype(jnp.float32))).reshape(
        seq_count, local_heads, head_dim
    )
    own_keys = lax.dynamic_slice_in_dim(new_keys, row_start, rows_here, 2)
    own_query = lax.dynamic_slice_in_dim(
        new_query.astype(jnp.float32).reshape(seq_count, local_heads, head_dim),
        row_start,
        rows_here,
        2,
    )
    value_new = new_value.astype(jnp.float32).reshape(seq_count, local_heads, head_dim)
    updated = (1.0 - own_keys)[..., None] * cache_rows.astype(jnp.float32) + own_keys[
        ..., None
    ] * value_new[:, :, None, :]
    read_part = jnp.einsum("sha,shab->shb", own_query, updated, precision=lax.Precision.HIGHEST)
    read_sum = of_everyone(read_part, "sp")
    scaled = (
        read_sum
        * lax.rsqrt(jnp.mean(read_sum * read_sum, axis=-1, keepdims=True) + 1e-06)
        * read_norm_scale
    )
    first_read = (
        scaled.reshape(seq_count, channels) * jax.nn.silu(new_gate.astype(jnp.float32))
    ).astype(jnp.bfloat16)
    return (cache_rows, first_read)


def solution(mesh):
    placed = (
        P("gr", "sp", "tp"),
        P("gr", "sp"),
        P(None, "tp"),
        P(None, "tp"),
        P("sp", "tp"),
        P("sp", "tp"),
        P("tp"),
        P("gr", "sp", "tp"),
        P(),
    )
    return jax.shard_map(
        per_device,
        mesh=mesh,
        in_specs=placed,
        out_specs=(P("gr", "tp", "sp", None), P("gr", "tp")),
        check_vma=False,
    )
```

profile of v0, /device:TPU:2, one launch (start us, length us, event | category | flops | bytes accessed | tf_op | source)
XLA Modules:
  0.0 156.7 jit_solution(15677566617659732985)
XLA Ops:
  7.2 0.0 copy-start
  7.2 0.0 copy-start.4
  7.2 0.0 all-gather.2.cloned.1.call-start
  7.2 0.7 all-gather.2.cloned.1.call-update
  7.9 0.2 copy-done
  8.1 0.8 convolution_bitcast_fusion.3
  8.9 1.1 convolution_bitcast_fusion.2
  10.1 1.1 convolution_bitcast_fusion.1
  11.2 1.1 convolution_bitcast_fusion
  12.3 0.2 copy.30
  12.5 1.0 broadcast_in_dim.20
  13.5 1.8 %reshape.149 = f32[4,192,512]{2,1,0:T(8,128)} reshape(f32[4,192,4,128]{3,2,1,0:T(4,128)S(1)} %broadcast_in_dim.20) | data formatting | bytes 3145728 | tf_op jit(solution)/shard_map/reshape | solution.py:88
  15.3 40.1 %all-gather.2.cloned.1.call-done = bf16[768,4096]{1,0:T(8,128)(2,1)} async-done(((bf16[768,512]{1,0:T(8,128)(2,1)}), bf16[768,4096]{1,0:T(8,128)(2,1)}) %all-gather.2.cloned.1.call-update) | async-done | bytes 6291472 | tf_op jit(solution)/shard_map/all_gather | solution.py:79
  55.3 7.4 %convolution_convert_fusion = bf16[768,512]{1,0:T(8,128)(2,1)S(1)} fusion(bf16[768,4096]{1,0:T(8,128)(2,1)} %all-gather.2.cloned.1.call-done, bf16[4096,512]{1,0:T(8,128)(2,1)} %param.12), kind=kOutput, calls=%fused_computation.10 | convolution fusion | flops 3221618688 | bytes 11272192 | tf_op jit(solution)/shard_map/dot_general | solution.py:81
  62.7 1.1 reshape.153
  63.9 7.0 %add_divide_fusion = f32[768,512]{1,0:T(8,128)S(1)} fusion(bf16[768,4096]{1,0:T(8,128)(2,1)} %all-gather.2.cloned.1.call-done, bf16[4096,512]{1,0:T(8,128)(2,1)} %param.11), kind=kOutput, calls=%fused_computation.9 | convolution fusion | flops 3222798336 | bytes 12058624 | tf_op jit(solution)/shard_map/dot_general | solution.py:80
  70.8 0.0 copy-start.5
  70.8 0.5 div.22
  71.4 0.1 copy-done.5
  71.5 2.4 %add_reduce_fusion = f32[4,4,128]{2,1,0:T(4,128)S(1)} fusion(f32[4,192,4,128]{3,2,1,0:T(4,128)S(1)} %div.22, f32[4,192,4]{2,1,0:T(8,128)} %copy-done.2, f32[4,128]{1,0:T(4,128)S(1)} %bitcast.77), kind=kLoop, calls=%fused_computation.8 | loop fusion | flops 1570816 | bytes 1595392 | tf_op jit(solution)/shard_map/reduce_sum | solution.py:91
  73.9 0.7 broadcast_in_dim.22
  74.6 7.4 %all-to-all-start = ((f32[16,4,512]{2,1,0:T(4,128)}), f32[16,4,512]{2,1,0:T(4,128)S(1)}, u32[]{:S(2)}, u32[]{:S(2)}) async-start(f32[16,4,512]{2,1,0:T(4,128)} %broadcast_in_dim.22), calls=%async_computation | async-start | bytes 262144 | tf_op jit(solution)/shard_map/all_to_all | solution.py:9
  82.0 2.0 %add_bitcast_fusion = f32[4,512,192]{1,2,0:T(8,128)S(1)} fusion(f32[4,192,512]{2,1,0:T(8,128)} %reshape.149, f32[4,192,512]{2,1,0:T(8,128)S(1)} %bitcast.70, f32[512]{0:T(512)S(1)} %copy-done.5), kind=kLoop, calls=%fused_computation.7 | loop fusion | flops 1179648 | bytes 4720640 | tf_op jit(solution)/shard_map/transpose
  84.0 0.3 pad.3
  84.3 1.6 %fusion = f32[4,512,2,128]{1,2,3,0:T(2,128)S(1)} fusion(f32[4,512,2,128]{1,3,2,0:T(8,128)S(1)} %bitcast.72), kind=kOutput, calls=%fused_computation | output fusion | flops 66584576 | bytes 4194304 | tf_op jit(solution)/shard_map/reduce-window
  85.9 1.3 copy-done.1
  87.3 0.1 reduce-window.9
  87.3 2.3 %broadcast_add_fusion = f32[4,512,2,128]{1,2,3,0:T(2,128)S(1)} fusion(f32[4,512,2,128]{1,2,3,0:T(2,128)} %copy-done.1, f32[4,512,2]{1,2,0:T(2,128)S(1)} %slice.107), kind=kLoop, calls=%fused_computation.18 | loop fusion | flops 524288 | bytes 4210688 | tf_op jit(solution)/shard_map/reduce_window_sum
  89.7 1.7 %copy.32 = f32[4,512,2,128]{1,3,2,0:T(8,128)} copy(f32[4,512,2,128]{1,2,3,0:T(2,128)S(1)} %broadcast_add_fusion) | data formatting | bytes 4194304 | tf_op jit(solution)/shard_map/reduce_window_sum
  91.4 1.2 broadcast_in_dim.24
  92.6 7.5 %all-to-all-start.2 = ((f32[16,1,8192]{2,1,0:T(1,128)}), f32[16,1,8192]{2,1,0:T(1,128)S(1)}, u32[]{:S(2)}, u32[]{:S(2)}) async-start(f32[16,1,8192]{2,1,0:T(1,128)} %broadcast_in_dim.24), calls=%async_computation.2 | async-start | bytes 1048576 | tf_op jit(solution)/shard_map/all_to_all | solution.py:9
  100.1 0.1 broadcast_select_fusion
  100.3 2.1 %fusion.6 = bf16[4,4,16,8,128]{4,3,2,1,0:T(8,128)(2,1)S(1)} fusion(bf16[4,192,4,128]{3,2,1,0:T(4,128)(2,1)S(1)} %copy-done.3, f32[4,256,512]{2,1,0:T(8,128)} %bitcast.73, f32[4,192,512]{2,1,0:T(8,128)S(1)} %bitcast.71, f32[4,512]{1,0:T(4,128)S(1)} %fusion.22, f32[4,512]{1,0:T(4,128)S(1)} %bitcast.76, f32[512]{0:T(512)S(1)} %copy-done.5), kind=kOutput, calls=%fused_computation.13 | convolution fusion | flops 102891520 | bytes 4474880 | tf_op jit(solution)/shard_map/slha,slhb->shab/dot_general | solution.py:96
  102.4 0.9 copy.64
  103.3 12.0 %all-to-all-done.2 = f32[16,1,8192]{2,1,0:T(1,128)S(1)} async-done(((f32[16,1,8192]{2,1,0:T(1,128)}), f32[16,1,8192]{2,1,0:T(1,128)S(1)}, u32[]{:S(2)}, u32[]{:S(2)}) %all-to-all-start.2) | async-done | bytes 524320 | tf_op jit(solution)/shard_map/all_to_all | solution.py:9
  115.3 4.6 %all-to-all-start.1 = ((bf16[16,4,4,8,128]{4,3,2,1,0:T(8,128)(2,1)}), bf16[16,4,4,8,128]{4,3,2,1,0:T(8,128)(2,1)S(1)}, u32[]{:S(2)}, u32[]{:S(2)}) async-start(bf16[16,4,4,8,128]{4,3,2,1,0:T(8,128)(2,1)} %bitcast.68), calls=%async_computation.1 | async-start | bytes 1048576 | tf_op jit(solution)/shard_map/all_to_all | solution.py:42
  120.0 0.4 reduce_sum.50
  120.5 0.1 dynamic-slice_bitcast_fusion
  120.5 0.1 broadcast_subtract_fusion
  120.6 14.1 %all-to-all-done.1 = bf16[16,4,4,8,128]{4,3,2,1,0:T(8,128)(2,1)S(1)} async-done(((bf16[16,4,4,8,128]{4,3,2,1,0:T(8,128)(2,1)}), bf16[16,4,4,8,128]{4,3,2,1,0:T(8,128)(2,1)S(1)}, u32[]{:S(2)}, u32[]{:S(2)}) %all-to-all-start.1) | async-done | bytes 524320 | tf_op jit(solution)/shard_map/all_to_all | solution.py:42
  134.7 0.1 reduce_sum.49
  134.8 0.3 fusion.13
  135.0 0.7 broadcast_in_dim.25
  135.7 4.4 %all-to-all-start.3 = ((f32[16,4,4,128]{3,2,1,0:T(4,128)}), f32[16,4,4,128]{3,2,1,0:T(4,128)S(1)}, u32[]{:S(2)}, u32[]{:S(2)}) async-start(f32[16,4,4,128]{3,2,1,0:T(4,128)} %broadcast_in_dim.25), calls=%async_computation.3 | async-start | bytes 262144 | tf_op jit(solution)/shard_map/all_to_all | solution.py:9
  140.2 8.9 %all-to-all-done.3 = f32[16,4,4,128]{3,2,1,0:T(4,128)S(1)} async-done(((f32[16,4,4,128]{3,2,1,0:T(4,128)}), f32[16,4,4,128]{3,2,1,0:T(4,128)S(1)}, u32[]{:S(2)}, u32[]{:S(2)}) %all-to-all-start.3) | async-done | bytes 131104 | tf_op jit(solution)/shard_map/all_to_all | solution.py:9
  149.1 0.1 multiply_reduce_fusion
  149.2 0.1 multiply_bitcast_fusion
  149.3 0.6 fusion.24
  (37 shorter events, 0.2 us)
Async XLA Ops:
  7.2 1.0 copy-start
  7.2 4.0 %copy-start.4 = (bf16[4,256]{1,0:T(4,128)(2,1)S(1)}, bf16[4,256]{1,0:T(4,128)(2,1)}, u32[]{:S(2)}) copy-start(bf16[4,256]{1,0:T(4,128)(2,1)} %param.10) | copy-start | bytes 6148
  7.2 5.1 %copy-start.7 = (f32[4,192,4]{1,2,0:T(4,128)S(1)}, f32[4,192,4]{1,2,0:T(4,128)}, u32[]{:S(2)}) copy-start(f32[4,192,4]{1,2,0:T(4,128)} %param.16) | copy-start | bytes 36868
  7.2 48.1 %all-gather.2.cloned.1.call-start = ((), (), s32[]{:S(2)}) async-start(), calls=%async_computation.4 | async-start | bytes 7077888 | tf_op jit(solution)/shard_map/all_gather | solution.py:79
  12.5 2.8 %copy-start.2 = (f32[4,192,4]{2,1,0:T(8,128)}, f32[4,192,4]{2,1,0:T(8,128)S(1)}, u32[]{:S(2)}) copy-start(f32[4,192,4]{2,1,0:T(8,128)S(1)} %copy.30) | copy-start | bytes 36868
  70.8 0.7 copy-start.5
  74.6 16.8 %all-to-all-start = ((f32[16,4,512]{2,1,0:T(4,128)}), f32[16,4,512]{2,1,0:T(4,128)S(1)}, u32[]{:S(2)}, u32[]{:S(2)}) async-start(f32[16,4,512]{2,1,0:T(4,128)} %broadcast_in_dim.22), calls=%async_computation | async-start | bytes 262144 | tf_op jit(solution)/shard_map/all_to_all | solution.py:9
  85.9 1.3 copy-start.1
  91.4 8.9 %copy-start.3 = (bf16[4,192,4,128]{3,2,1,0:T(4,128)(2,1)S(1)}, bf16[4,192,4,128]{3,2,1,0:T(4,128)(2,1)}, u32[]{:S(2)}) copy-start(bf16[4,192,4,128]{3,2,1,0:T(4,128)(2,1)} %reshape.153) | copy-start | bytes 2359300
  92.6 22.8 %all-to-all-start.2 = ((f32[16,1,8192]{2,1,0:T(1,128)}), f32[16,1,8192]{2,1,0:T(1,128)S(1)}, u32[]{:S(2)}, u32[]{:S(2)}) async-start(f32[16,1,8192]{2,1,0:T(1,128)} %broadcast_in_dim.24), calls=%async_computation.2 | async-start | bytes 1048576 | tf_op jit(solution)/shard_map/all_to_all | solution.py:9
  115.3 24.8 %copy-start.8 = (f32[128]{0:T(128)S(1)}, f32[128]{0:T(128)}, u32[]{:S(2)}) copy-start(f32[128]{0:T(128)} %param.17) | copy-start | bytes 1540
  115.3 19.3 %all-to-all-start.1 = ((bf16[16,4,4,8,128]{4,3,2,1,0:T(8,128)(2,1)}), bf16[16,4,4,8,128]{4,3,2,1,0:T(8,128)(2,1)S(1)}, u32[]{:S(2)}, u32[]{:S(2)}) async-start(bf16[16,4,4,8,128]{4,3,2,1,0:T(8,128)(2,1)} %bitcast.68), calls=%async_computation.1 | async-start | bytes 1048576 | tf_op jit(solution)/shard_map/all_to_all | solution.py:42
  134.8 15.1 %copy-start.6 = (bf16[4,4,8,128]{3,2,1,0:T(8,128)(2,1)}, bf16[4,4,8,128]{3,2,1,0:T(8,128)(2,1)S(1)}, u32[]{:S(2)}) copy-start(bf16[4,4,8,128]{3,2,1,0:T(8,128)(2,1)S(1)} %reduce_sum.49) | copy-start | bytes 98308
  135.7 13.4 %all-to-all-start.3 = ((f32[16,4,4,128]{3,2,1,0:T(4,128)}), f32[16,4,4,128]{3,2,1,0:T(4,128)S(1)}, u32[]{:S(2)}, u32[]{:S(2)}) async-start(f32[16,4,4,128]{3,2,1,0:T(4,128)} %broadcast_in_dim.25), calls=%async_computation.3 | async-start | bytes 262144 | tf_op jit(solution)/shard_map/all_to_all | solution.py:9
Sparse Core Ops, SparseCore 0:
  9.8 45.4 all-gather.1
where the time goes:
time: 157 us
  waiting for transfers between devices  75.7 us (48%)
  starting transfers between devices  24 us (15%)
  matrix products  20.8 us (13%)
  between operations  14.3 us (9%)
  local copies, waits for them, and re-layouts  11.9 us (8%)
  other arithmetic  10 us (6%)
    all_gather x1, waiting for transfers between devices, per_device(): segment = lax.all_gather(flat_rows, 'tp', axis=1, tiled=True)  40.1 us
    all_to_all x3, waiting for transfers between devices, from_everyone(): lax.all_to_all(jnp.broadcast_to(shard[None], (count, *shard.shape)), axis...  20.9 us
    all_to_all x3, starting transfers between devices, from_everyone(): lax.all_to_all(jnp.broadcast_to(shard[None], (count, *shard.shape)), axis...  19.3 us
    all_to_all x1, waiting for transfers between devices, sent_and_summed(): lax.all_to_all(cut_along(shard, dim, count), axis, 0, 0, tiled=True)  14.1 us
    dot_general x1, matrix products, per_device(): jnp.dot(segment, value_weight, preferred_element_type=jnp.float32)  7.4 us
    dot_general x1, matrix products, per_device(): jnp.dot(segment, forget_weight, preferred_element_type=jnp.float32)  6.97 us
    all_to_all x1, starting transfers between devices, sent_and_summed(): lax.all_to_all(cut_along(shard, dim, count), axis, 0, 0, tiled=True)  4.63 us
    another operation x3, other arithmetic  4.02 us
  transfers between devices with their start and end apart: 5, of which 4 were waited for; matrix products, arithmetic and copies ran while one was open for 12% of the time, Pallas kernels for 0%

commit v1 on v0

--- a/solution.py
+++ b/solution.py
@@ -2,6 +2,27 @@
 import jax.numpy as jnp
 from jax import lax
 from jax.sharding import PartitionSpec as P
+
+
+def gather_around(shard, axis, dim):
+    devices, index, rows = (lax.axis_size(axis), lax.axis_index(axis), shard.shape[dim])
+    ahead = [(i, (i + 1) % devices) for i in range(devices)]
+    left = [(i, (i - 1) % devices) for i in range(devices)]
+    whole = jnp.zeros((*shard.shape[:dim], devices * rows, *shard.shape[dim + 1 :]), shard.dtype)
+    whole = lax.dynamic_update_slice_in_dim(whole, shard, index * rows, axis=dim)
+    from_left = from_right = shard
+    halfway = devices // 2
+    for lap in range(1, halfway + 1):
+        from_left = lax.ppermute(from_left, axis, ahead)
+        whole = lax.dynamic_update_slice_in_dim(
+            whole, from_left, (index - lap) % devices * rows, axis=dim
+        )
+        if lap < devices - halfway:
+            from_right = lax.ppermute(from_right, axis, left)
+            whole = lax.dynamic_update_slice_in_dim(
+                whole, from_right, (index + lap) % devices * rows, axis=dim
+            )
+    return whole
 
 
 def from_everyone(shard, axis):
@@ -76,7 +97,7 @@
     local_heads = additional_damping_exponent.shape[2]
     channels = local_heads * head_dim
     flat_rows = tokens.reshape(seq_count * block_len, width_part)
-    segment = lax.all_gather(flat_rows, "tp", axis=1, tiled=True)
+    segment = gather_around(flat_rows, "tp", 1)
     forget_acc = jnp.dot(segment, forget_weight, preferred_element_type=jnp.float32)
     value_acc = jnp.dot(segment, value_weight, preferred_element_type=jnp.float32)
     forget = forget_acc.astype(jnp.bfloat16).reshape(seq_count, block_len, channels)

time: 157 us -> 139 us (0.89)
  the two profiles are of different devices: /device:TPU:2 before, /device:TPU:6 now
where the time goes in v1:
time: 139 us; the launch traced here: 138 us
  waiting for transfers between devices  63.7 us (46%)
  starting transfers between devices  32.9 us (24%)
  local copies, waits for them, and re-layouts  17.3 us (12%)
  matrix products  12.8 us (9%)
  other arithmetic  10.6 us (8%)
    ppermute x4, waiting for transfers between devices, gather_around(): from_left = lax.ppermute(from_left, axis, ahead)  26.6 us
    all_to_all x3, waiting for transfers between devices, from_everyone(): lax.all_to_all(jnp.broadcast_to(shard[None], (count, *shard.shape)), axis...  22.1 us
    all_to_all x3, starting transfers between devices, from_everyone(): lax.all_to_all(jnp.broadcast_to(shard[None], (count, *shard.shape)), axis...  20.6 us
    all_to_all x1, waiting for transfers between devices, sent_and_summed(): lax.all_to_all(cut_along(shard, dim, count), axis, 0, 0, tiled=True)  15 us
    all_to_all x1, starting transfers between devices, sent_and_summed(): lax.all_to_all(cut_along(shard, dim, count), axis, 0, 0, tiled=True)  4.52 us
    ppermute x3, starting transfers between devices, gather_around(): from_right = lax.ppermute(from_right, axis, left)  4.4 us
    dot_general x1, matrix products, per_device(): jnp.dot(segment, value_weight, preferred_element_type=jnp.float32)  4.34 us
    another operation x3, other arithmetic  4.01 us
  transfers between devices with their start and end apart: 11, of which 7 were waited for; matrix products, arithmetic and copies ran while one was open for 17% of the time, Pallas kernels for 0%

profile of v1, /device:TPU:6, one launch (start us, length us, event | category | flops | bytes accessed | tf_op | source)
XLA Modules:
  0.0 138.4 jit_solution(15363405005871037140)
XLA Ops:
  0.7 1.7 %collective-permute-start.1 = (bf16[768,512]{1,0:T(8,128)(2,1)}, bf16[768,512]{1,0:T(8,128)(2,1)}, u32[]{:S(2)}, u32[]{:S(2)}) collective-permute-start(bf16[768,512]{1,0:T(8,128)(2,1)} %bitcast.75), channel_id=1, source_target_pairs={{0,7},{1,0},{2,1},{3,2},{4,3},{5,4},{6,5},{7,6},{8,15},{9,8},{10,9... | collective-permute-start | bytes 2359304 | tf_op jit(solution)/shard_map/ppermute | solution.py:21
  2.4 9.9 %collective-permute-done = bf16[768,512]{1,0:T(8,128)(2,1)S(1)} collective-permute-done((bf16[768,512]{1,0:T(8,128)(2,1)}, bf16[768,512]{1,0:T(8,128)(2,1)S(1)}, u32[]{:S(2)}, u32[]{:S(2)}) %collective-permute-start) | collective-permute-done | bytes 786464 | tf_op jit(solution)/shard_map/ppermute | solution.py:16
  12.3 1.8 %collective-permute-start.3 = (bf16[768,512]{1,0:T(8,128)(2,1)}, bf16[768,512]{1,0:T(8,128)(2,1)}, u32[]{:S(2)}, u32[]{:S(2)}) collective-permute-start(bf16[768,512]{1,0:T(8,128)(2,1)} %collective-permute-done.1), channel_id=1, source_target_pairs={{0,7},{1,0},{2,1},{3,2},{4,3},{5,4},{6,5},{7,6},{8,15},{9,8},{10,9... | collective-permute-start | bytes 2359304 | tf_op jit(solution)/shard_map/ppermute | solution.py:21
  14.1 0.9 copy.30
  15.1 1.0 broadcast_in_dim.23
  16.0 1.8 %reshape.149 = f32[4,192,512]{2,1,0:T(8,128)} reshape(f32[4,192,4,128]{3,2,1,0:T(4,128)S(1)} %broadcast_in_dim.23) | data formatting | bytes 3145728 | tf_op jit(solution)/shard_map/reshape | solution.py:109
  17.8 6.0 %collective-permute-done.2 = bf16[768,512]{1,0:T(8,128)(2,1)} collective-permute-done((bf16[768,512]{1,0:T(8,128)(2,1)S(1)}, bf16[768,512]{1,0:T(8,128)(2,1)}, u32[]{:S(2)}, u32[]{:S(2)}) %collective-permute-start.2) | collective-permute-done | bytes 786464 | tf_op jit(solution)/shard_map/ppermute | solution.py:16
  23.8 0.9 collective-permute-start.4
  24.7 1.1 convolution_bitcast_fusion.1
  25.8 1.1 convolution_bitcast_fusion
  26.9 0.1 convolution_bitcast_fusion.3
  27.1 0.1 convolution_bitcast_fusion.2
  27.3 0.6 pad_maximum_fusion
  27.9 0.8 collective-permute-start.5
  28.7 0.8 broadcast_in_dim.22
  29.6 5.8 %collective-permute-done.4 = bf16[768,512]{1,0:T(8,128)(2,1)S(1)} collective-permute-done((bf16[768,512]{1,0:T(8,128)(2,1)}, bf16[768,512]{1,0:T(8,128)(2,1)S(1)}, u32[]{:S(2)}, u32[]{:S(2)}) %collective-permute-start.4) | collective-permute-done | bytes 786464 | tf_op jit(solution)/shard_map/ppermute | solution.py:16
  35.4 2.3 %collective-permute-start.6 = (bf16[768,512]{1,0:T(8,128)(2,1)S(1)}, bf16[768,512]{1,0:T(8,128)(2,1)S(1)}, u32[]{:S(2)}, u32[]{:S(2)}) collective-permute-start(bf16[768,512]{1,0:T(8,128)(2,1)S(1)} %collective-permute-done.4), channel_id=1, source_target_pairs={{0,1},{1,2},{2,3},{3,4},{4,5},{5,6},{6,7},{7,0},{8,9},{9,10},{10,1... | collective-permute-start | bytes 2359304 | tf_op jit(solution)/shard_map/ppermute | solution.py:16
  37.9 1.2 constant_dynamic-update-slice_fusion.5
  39.1 1.2 constant_dynamic-update-slice_fusion.4
  40.4 1.2 constant_dynamic-update-slice_fusion.3
  41.9 4.9 %collective-permute-done.6 = bf16[768,512]{1,0:T(8,128)(2,1)S(1)} collective-permute-done((bf16[768,512]{1,0:T(8,128)(2,1)S(1)}, bf16[768,512]{1,0:T(8,128)(2,1)S(1)}, u32[]{:S(2)}, u32[]{:S(2)}) %collective-permute-start.6) | collective-permute-done | bytes 786464 | tf_op jit(solution)/shard_map/ppermute | solution.py:16
  47.0 3.6 %add_divide_fusion = f32[768,512]{1,0:T(8,128)S(1)} fusion(bf16[768,4096]{1,0:T(8,128)(2,1)S(1)} %constant_dynamic-update-slice_fusion, bf16[4096,512]{1,0:T(8,128)(2,1)S(1)} %copy-done.9), kind=kOutput, calls=%fused_computation.9 | convolution fusion | flops 3222798336 | bytes 12058624 | tf_op jit(solution)/shard_map/dot_general | solution.py:101
  50.6 4.3 %convolution_convert_fusion = bf16[768,512]{1,0:T(8,128)(2,1)} fusion(bf16[768,4096]{1,0:T(8,128)(2,1)S(1)} %constant_dynamic-update-slice_fusion, bf16[4096,512]{1,0:T(8,128)(2,1)S(1)} %copy-done.10), kind=kOutput, calls=%fused_computation.10 | convolution fusion | flops 3221618688 | bytes 11272192 | tf_op jit(solution)/shard_map/dot_general | solution.py:102
  55.0 0.5 div.22
  55.5 0.1 copy-done.7
  55.6 2.4 %add_reduce_fusion = f32[4,4,128]{2,1,0:T(4,128)S(1)} fusion(f32[4,192,4,128]{3,2,1,0:T(4,128)S(1)} %div.22, f32[4,192,4]{2,1,0:T(8,128)} %copy-done.2, f32[4,128]{1,0:T(4,128)S(1)} %bitcast.79), kind=kLoop, calls=%fused_computation.8 | loop fusion | flops 1570816 | bytes 1595392 | tf_op jit(solution)/shard_map/reduce_sum | solution.py:112
  58.1 0.7 broadcast_in_dim.25
  58.7 8.6 %all-to-all-start = ((f32[16,4,512]{2,1,0:T(4,128)}), f32[16,4,512]{2,1,0:T(4,128)S(1)}, u32[]{:S(2)}, u32[]{:S(2)}) async-start(f32[16,4,512]{2,1,0:T(4,128)} %broadcast_in_dim.25), calls=%async_computation | async-start | bytes 262144 | tf_op jit(solution)/shard_map/all_to_all | solution.py:30
  67.4 2.0 %add_bitcast_fusion = f32[4,512,192]{1,2,0:T(8,128)S(1)} fusion(f32[4,192,512]{2,1,0:T(8,128)} %reshape.149, f32[4,192,512]{2,1,0:T(8,128)S(1)} %bitcast.70, f32[512]{0:T(512)S(1)} %copy-done.7), kind=kLoop, calls=%fused_computation.7 | loop fusion | flops 1179648 | bytes 4720640 | tf_op jit(solution)/shard_map/transpose
  69.4 0.3 pad.3
  69.7 1.6 %fusion = f32[4,512,2,128]{1,2,3,0:T(2,128)S(1)} fusion(f32[4,512,2,128]{1,3,2,0:T(8,128)S(1)} %bitcast.72), kind=kOutput, calls=%fused_computation | output fusion | flops 66584576 | bytes 4194304 | tf_op jit(solution)/shard_map/reduce-window
  71.3 1.3 copy-done.1
  72.7 2.3 %broadcast_add_fusion = f32[4,512,2,128]{1,2,3,0:T(2,128)S(1)} fusion(f32[4,512,2,128]{1,2,3,0:T(2,128)} %copy-done.1, f32[4,512,2]{1,2,0:T(2,128)S(1)} %slice.107), kind=kLoop, calls=%fused_computation.18 | loop fusion | flops 524288 | bytes 4210688 | tf_op jit(solution)/shard_map/reduce_window_sum
  75.1 1.7 %copy.32 = f32[4,512,2,128]{1,3,2,0:T(8,128)} copy(f32[4,512,2,128]{1,2,3,0:T(2,128)S(1)} %broadcast_add_fusion) | data formatting | bytes 4194304 | tf_op jit(solution)/shard_map/reduce_window_sum
  76.8 0.2 reshape.153
  77.0 2.0 %broadcast_in_dim.27 = f32[16,1,8192]{2,1,0:T(1,128)} broadcast(f32[8192]{0:T(1024)} %pad_maximum_fusion), dimensions={2} | broadcast | bytes 557056 | tf_op jit(solution)/shard_map/broadcast_in_dim | solution.py:31
  79.0 7.5 %all-to-all-start.2 = ((f32[16,1,8192]{2,1,0:T(1,128)}), f32[16,1,8192]{2,1,0:T(1,128)S(1)}, u32[]{:S(2)}, u32[]{:S(2)}) async-start(f32[16,1,8192]{2,1,0:T(1,128)} %broadcast_in_dim.27), calls=%async_computation.2 | async-start | bytes 1048576 | tf_op jit(solution)/shard_map/all_to_all | solution.py:30
  86.7 2.1 %fusion.6 = bf16[4,4,16,8,128]{4,3,2,1,0:T(8,128)(2,1)S(1)} fusion(bf16[4,192,4,128]{3,2,1,0:T(4,128)(2,1)S(1)} %reshape.153, f32[4,256,512]{2,1,0:T(8,128)} %bitcast.73, f32[4,192,512]{2,1,0:T(8,128)S(1)} %bitcast.71, f32[4,512]{1,0:T(4,128)S(1)} %fusion.22, f32[4,512]{1,0:T(4,128)S(1)} %bitcast.78, f32[512]{0:T(512)S(1)} %copy-done.7), kind=kOutput, calls=%fused_computation.13 | convolution fusion | flops 102891520 | bytes 4474880 | tf_op jit(solution)/shard_map/slha,slhb->shab/dot_general | solution.py:117
  88.8 0.9 copy.64
  89.7 13.3 %all-to-all-done.2 = f32[16,1,8192]{2,1,0:T(1,128)S(1)} async-done(((f32[16,1,8192]{2,1,0:T(1,128)}), f32[16,1,8192]{2,1,0:T(1,128)S(1)}, u32[]{:S(2)}, u32[]{:S(2)}) %all-to-all-start.2) | async-done | bytes 524320 | tf_op jit(solution)/shard_map/all_to_all | solution.py:30
  103.0 4.5 %all-to-all-start.1 = ((bf16[16,4,4,8,128]{4,3,2,1,0:T(8,128)(2,1)}), bf16[16,4,4,8,128]{4,3,2,1,0:T(8,128)(2,1)S(1)}, u32[]{:S(2)}, u32[]{:S(2)}) async-start(bf16[16,4,4,8,128]{4,3,2,1,0:T(8,128)(2,1)} %bitcast.68), calls=%async_computation.1 | async-start | bytes 1048576 | tf_op jit(solution)/shard_map/all_to_all | solution.py:63
  107.5 0.4 reduce_sum.50
  108.1 15.0 %all-to-all-done.1 = bf16[16,4,4,8,128]{4,3,2,1,0:T(8,128)(2,1)S(1)} async-done(((bf16[16,4,4,8,128]{4,3,2,1,0:T(8,128)(2,1)}), bf16[16,4,4,8,128]{4,3,2,1,0:T(8,128)(2,1)S(1)}, u32[]{:S(2)}, u32[]{:S(2)}) %all-to-all-start.1) | async-done | bytes 524320 | tf_op jit(solution)/shard_map/all_to_all | solution.py:63
  123.2 0.3 fusion.13
  123.4 0.7 broadcast_in_dim.28
  124.1 4.5 %all-to-all-start.3 = ((f32[16,4,4,128]{3,2,1,0:T(4,128)}), f32[16,4,4,128]{3,2,1,0:T(4,128)S(1)}, u32[]{:S(2)}, u32[]{:S(2)}) async-start(f32[16,4,4,128]{3,2,1,0:T(4,128)} %broadcast_in_dim.28), calls=%async_computation.3 | async-start | bytes 262144 | tf_op jit(solution)/shard_map/all_to_all | solution.py:30
  128.6 8.9 %all-to-all-done.3 = f32[16,4,4,128]{3,2,1,0:T(4,128)S(1)} async-done(((f32[16,4,4,128]{3,2,1,0:T(4,128)}), f32[16,4,4,128]{3,2,1,0:T(4,128)S(1)}, u32[]{:S(2)}, u32[]{:S(2)}) %all-to-all-start.3) | async-done | bytes 131104 | tf_op jit(solution)/shard_map/all_to_all | solution.py:30
  137.7 0.6 fusion.24
  (63 shorter events, 1.4 us)
Async XLA Ops:
  0.6 26.3 %copy-start = (bf16[256,512]{1,0:T(8,128)(2,1)S(1)}, bf16[256,512]{1,0:T(8,128)(2,1)}, u32[]{:S(2)}) copy-start(bf16[256,512]{1,0:T(8,128)(2,1)} %param.13) | copy-start | bytes 786436
  0.6 11.6 %collective-permute-start = (bf16[768,512]{1,0:T(8,128)(2,1)}, bf16[768,512]{1,0:T(8,128)(2,1)S(1)}, u32[]{:S(2)}, u32[]{:S(2)}) collective-permute-start(bf16[768,512]{1,0:T(8,128)(2,1)} %bitcast.74), channel_id=1, source_target_pairs={{0,1},{1,2},{2,3},{3,4},{4,5},{5,6},{6,7},{7,0},{8,9},{9,10},{10,1... | collective-permute-start | bytes 2359304 | tf_op jit(solution)/shard_map/ppermute | solution.py:16
  0.7 11.6 %collective-permute-start.1 = (bf16[768,512]{1,0:T(8,128)(2,1)}, bf16[768,512]{1,0:T(8,128)(2,1)}, u32[]{:S(2)}, u32[]{:S(2)}) collective-permute-start(bf16[768,512]{1,0:T(8,128)(2,1)} %bitcast.75), channel_id=1, source_target_pairs={{0,7},{1,0},{2,1},{3,2},{4,3},{5,4},{6,5},{7,6},{8,15},{9,8},{10,9... | collective-permute-start | bytes 2359304 | tf_op jit(solution)/shard_map/ppermute | solution.py:21
  12.3 11.5 %collective-permute-start.2 = (bf16[768,512]{1,0:T(8,128)(2,1)S(1)}, bf16[768,512]{1,0:T(8,128)(2,1)}, u32[]{:S(2)}, u32[]{:S(2)}) collective-permute-start(bf16[768,512]{1,0:T(8,128)(2,1)S(1)} %collective-permute-done), channel_id=1, source_target_pairs={{0,1},{1,2},{2,3},{3,4},{4,5},{5,6},{6,7},{7,0},{8,9},{9,10},{10,1... | collective-permute-start | bytes 2359304 | tf_op jit(solution)/shard_map/ppermute | solution.py:16
  12.3 15.6 %collective-permute-start.3 = (bf16[768,512]{1,0:T(8,128)(2,1)}, bf16[768,512]{1,0:T(8,128)(2,1)}, u32[]{:S(2)}, u32[]{:S(2)}) collective-permute-start(bf16[768,512]{1,0:T(8,128)(2,1)} %collective-permute-done.1), channel_id=1, source_target_pairs={{0,7},{1,0},{2,1},{3,2},{4,3},{5,4},{6,5},{7,6},{8,15},{9,8},{10,9... | collective-permute-start | bytes 2359304 | tf_op jit(solution)/shard_map/ppermute | solution.py:21
  15.0 2.8 %copy-start.2 = (f32[4,192,4]{2,1,0:T(8,128)}, f32[4,192,4]{2,1,0:T(8,128)S(1)}, u32[]{:S(2)}) copy-start(f32[4,192,4]{2,1,0:T(8,128)S(1)} %copy.30) | copy-start | bytes 36868
  15.0 9.7 %copy-start.6 = (bf16[4,256]{1,0:T(4,128)(2,1)S(1)}, bf16[4,256]{1,0:T(4,128)(2,1)}, u32[]{:S(2)}) copy-start(bf16[4,256]{1,0:T(4,128)(2,1)} %param.10) | copy-start | bytes 6148
  16.0 11.1 %copy-start.5 = (bf16[256,512]{1,0:T(8,128)(2,1)S(1)}, bf16[256,512]{1,0:T(8,128)(2,1)}, u32[]{:S(2)}) copy-start(bf16[256,512]{1,0:T(8,128)(2,1)} %param.14) | copy-start | bytes 786436
  23.8 11.6 %collective-permute-start.4 = (bf16[768,512]{1,0:T(8,128)(2,1)}, bf16[768,512]{1,0:T(8,128)(2,1)S(1)}, u32[]{:S(2)}, u32[]{:S(2)}) collective-permute-start(bf16[768,512]{1,0:T(8,128)(2,1)} %collective-permute-done.2), channel_id=1, source_target_pairs={{0,1},{1,2},{2,3},{3,4},{4,5},{5,6},{6,7},{7,0},{8,9},{9,10},{10,1... | collective-permute-start | bytes 2359304 | tf_op jit(solution)/shard_map/ppermute | solution.py:16
  27.9 1.6 %copy-start.3 = (bf16[4,192,512]{2,1,0:T(8,128)(2,1)S(1)}, bf16[4,192,512]{2,1,0:T(8,128)(2,1)}, u32[]{:S(2)}) copy-start(bf16[4,192,512]{2,1,0:T(8,128)(2,1)} %param.9) | copy-start | bytes 2359300
  27.9 13.9 %collective-permute-start.5 = (bf16[768,512]{1,0:T(8,128)(2,1)}, bf16[768,512]{1,0:T(8,128)(2,1)S(1)}, u32[]{:S(2)}, u32[]{:S(2)}) collective-permute-start(bf16[768,512]{1,0:T(8,128)(2,1)} %collective-permute-done.3), channel_id=1, source_target_pairs={{0,7},{1,0},{2,1},{3,2},{4,3},{5,4},{6,5},{7,6},{8,15},{9,8},{10,9... | collective-permute-start | bytes 2359304 | tf_op jit(solution)/shard_map/ppermute | solution.py:21
  35.4 11.4 %collective-permute-start.6 = (bf16[768,512]{1,0:T(8,128)(2,1)S(1)}, bf16[768,512]{1,0:T(8,128)(2,1)S(1)}, u32[]{:S(2)}, u32[]{:S(2)}) collective-permute-start(bf16[768,512]{1,0:T(8,128)(2,1)S(1)} %collective-permute-done.4), channel_id=1, source_target_pairs={{0,1},{1,2},{2,3},{3,4},{4,5},{5,6},{6,7},{7,0},{8,9},{9,10},{10,1... | collective-permute-start | bytes 2359304 | tf_op jit(solution)/shard_map/ppermute | solution.py:16
  41.6 5.3 %copy-start.9 = (bf16[4096,512]{1,0:T(8,128)(2,1)S(1)}, bf16[4096,512]{1,0:T(8,128)(2,1)}, u32[]{:S(2)}) copy-start(bf16[4096,512]{1,0:T(8,128)(2,1)} %param.11) | copy-start | bytes 12582916
  47.0 3.7 %copy-start.10 = (bf16[4096,512]{1,0:T(8,128)(2,1)S(1)}, bf16[4096,512]{1,0:T(8,128)(2,1)}, u32[]{:S(2)}) copy-start(bf16[4096,512]{1,0:T(8,128)(2,1)} %param.12) | copy-start | bytes 12582916
  55.0 0.7 copy-start.7
  58.7 18.2 %all-to-all-start = ((f32[16,4,512]{2,1,0:T(4,128)}), f32[16,4,512]{2,1,0:T(4,128)S(1)}, u32[]{:S(2)}, u32[]{:S(2)}) async-start(f32[16,4,512]{2,1,0:T(4,128)} %broadcast_in_dim.25), calls=%async_computation | async-start | bytes 262144 | tf_op jit(solution)/shard_map/all_to_all | solution.py:30
  71.3 1.3 copy-start.1
  75.1 1.7 %copy-start.4 = (bf16[768,512]{1,0:T(8,128)(2,1)S(1)}, bf16[768,512]{1,0:T(8,128)(2,1)}, u32[]{:S(2)}) copy-start(bf16[768,512]{1,0:T(8,128)(2,1)} %convolution_convert_fusion) | copy-start | bytes 2359300
  79.0 24.0 %all-to-all-start.2 = ((f32[16,1,8192]{2,1,0:T(1,128)}), f32[16,1,8192]{2,1,0:T(1,128)S(1)}, u32[]{:S(2)}, u32[]{:S(2)}) async-start(f32[16,1,8192]{2,1,0:T(1,128)} %broadcast_in_dim.27), calls=%async_computation.2 | async-start | bytes 1048576 | tf_op jit(solution)/shard_map/all_to_all | solution.py:30
  88.8 39.9 %copy-start.11 = (f32[128]{0:T(128)S(1)}, f32[128]{0:T(128)}, u32[]{:S(2)}) copy-start(f32[128]{0:T(128)} %param.17) | copy-start | bytes 1540
  103.0 20.1 %all-to-all-start.1 = ((bf16[16,4,4,8,128]{4,3,2,1,0:T(8,128)(2,1)}), bf16[16,4,4,8,128]{4,3,2,1,0:T(8,128)(2,1)S(1)}, u32[]{:S(2)}, u32[]{:S(2)}) async-start(bf16[16,4,4,8,128]{4,3,2,1,0:T(8,128)(2,1)} %bitcast.68), calls=%async_computation.1 | async-start | bytes 1048576 | tf_op jit(solution)/shard_map/all_to_all | solution.py:63
  123.2 15.2 %copy-start.8 = (bf16[4,4,8,128]{3,2,1,0:T(8,128)(2,1)}, bf16[4,4,8,128]{3,2,1,0:T(8,128)(2,1)S(1)}, u32[]{:S(2)}) copy-start(bf16[4,4,8,128]{3,2,1,0:T(8,128)(2,1)S(1)} %reduce_sum.49) | copy-start | bytes 98308
  124.1 13.4 %all-to-all-start.3 = ((f32[16,4,4,128]{3,2,1,0:T(4,128)}), f32[16,4,4,128]{3,2,1,0:T(4,128)S(1)}, u32[]{:S(2)}, u32[]{:S(2)}) async-start(f32[16,4,4,128]{3,2,1,0:T(4,128)} %broadcast_in_dim.28), calls=%async_computation.3 | async-start | bytes 262144 | tf_op jit(solution)/shard_map/all_to_all | solution.py:30
